TPU v7x, 32 devices: a whole 2x2x4 slice. The times are simulated.
32 devices in a mesh: sp: 8 (over z, x), tp: 4 (over y, core).
Axes of the slice: x: 2, y: 2, z: 4, core: 2. Of those that a mesh axis runs over, the one named last changes fastest.
Arguments:
- features: bfloat16 [3072, 2048], P('sp', 'tp'), may hold values from -6 to 6
- norm_gain: float32 [2048], replicated, may hold values from 0.28 to 10
- w_query: bfloat16 [2048, 1024], P(None, 'tp'), may hold values from -0.125 to 0.125
- w_key: bfloat16 [2048, 512], P(None, 'tp'), may hold values from -0.125 to 0.125
- w_value: bfloat16 [2048, 512], P(None, 'tp'), may hold values from -0.125 to 0.125
- head_sinks: float32 [16], P('tp'), may hold values from 1 to 5
- w_query_latent: bfloat16 [2048, 512], replicated, may hold values from -0.125 to 0.125
- w_kv_latent: bfloat16 [2048, 512], replicated, may hold values from -0.125 to 0.125
- w_rope_key: bfloat16 [2048, 64], replicated, may hold values from -0.125 to 0.125
- query_latent_gain: float32 [512], replicated, may hold values from 0.28 to 10
- kv_latent_gain: float32 [512], replicated, may hold values from 0.28 to 10
- w_query_content: bfloat16 [512, 1024], P(None, 'tp'), may hold values from -0.25 to 0.25
- w_query_rotary: bfloat16 [512, 512], P(None, 'tp'), may hold values from -0.25 to 0.25
- w_key_up: bfloat16 [512, 1024], P(None, 'tp'), may hold values from -0.25 to 0.25
- w_value_up: bfloat16 [512, 1024], P(None, 'tp'), may hold values from -0.25 to 0.25
- w_branch_window: bfloat16 [1024, 2048], P('tp'), may hold values from -0.1875 to 0.1875
- w_branch_latent: bfloat16 [1024, 2048], P('tp'), may hold values from -0.1875 to 0.1875
- w_gate_window: bfloat16 [2048, 2048], P(None, 'tp'), may hold values from -0.125 to 0.125
- w_gate_latent: bfloat16 [2048, 2048], P(None, 'tp'), may hold values from -0.125 to 0.125
Outputs:
- mixed: bfloat16 [3072, 2048], P('sp', 'tp')
All inputs are finite; a program needn't handle non-finite values.
Results may differ from a plain program's by a relative error of at most 0.018.
The roundings to bfloat16 on the way count: a program that leaves them out, or rounds other values in their place, can miss the bound.
Values may be sent and summed in bfloat16 or wider, within the bound.
A program may use at most 128 MiB of HBM per device.

v0:
```python
import jax
import jax.numpy as jnp
from jax import lax
from jax.sharding import PartitionSpec as P

HEAD = 64
WINDOW = 128
NOPE = 128
ROPE = 64
VDIM = 128
EPS = 1e-06
THETA = 10000.0
NEGATIVE = -1e30


def from_behind(shard, axis, by):
    count = lax.axis_size(axis)
    pairs = [(i, i + by) for i in range(count) if 0 <= i + by < count]
    return lax.ppermute(shard, axis, pairs)


def rms_rows(float_rows, gain_vec):
    return (
        float_rows
        * lax.rsqrt(jnp.mean(float_rows * float_rows, axis=-1, keepdims=True) + EPS)
        * gain_vec
    )


def rotate(float_rows, positions):
    half_width = float_rows.shape[-1] // 2
    frequencies = THETA ** (-jnp.arange(half_width, dtype=jnp.float32) / half_width)
    angles = positions.astype(jnp.float32)[:, None] * frequencies
    target = (float_rows.shape[0],) + (1,) * (float_rows.ndim - 2) + (half_width,)
    cosine = jnp.cos(angles).reshape(target)
    sine_part = jnp.sin(angles).reshape(target)
    first_half = float_rows[..., :half_width]
    second_half = float_rows[..., half_width:]
    return jnp.concatenate(
        [
            first_half * cosine - second_half * sine_part,
            second_half * cosine + first_half * sine_part,
        ],
        axis=-1,
    )


def project(left, right):
    return jnp.dot(left, right, preferred_element_type=jnp.float32)


def window_attention(queries, key_ext, value_ext, sink_table, row_start):
    row_count = queries.shape[0]
    kv_heads = key_ext.shape[1] // HEAD
    group_size = queries.shape[1] // HEAD // kv_heads
    blocks = row_count // WINDOW
    query_blocks = queries.reshape(blocks, WINDOW, kv_heads, group_size, HEAD)

    def banded(table):
        table = table.reshape(blocks + 1, WINDOW, kv_heads, HEAD)
        return jnp.concatenate([table[:-1], table[1:]], axis=1)

    key_band = banded(key_ext)
    value_band = banded(value_ext)
    scores = jnp.einsum(
        "nqhgd,nkhd->nhgqk", query_blocks, key_band, preferred_element_type=jnp.float32
    ) * HEAD ** (-0.5)
    query_index = jnp.arange(WINDOW, dtype=jnp.int32)[:, None]
    key_index = jnp.arange(2 * WINDOW, dtype=jnp.int32)[None, :]
    offset = query_index + WINDOW - key_index
    key_position = (
        row_start + jnp.arange(blocks, dtype=jnp.int32)[:, None, None] * WINDOW + key_index - WINDOW
    )
    valid_mask = ((offset >= 0) & (offset < WINDOW) & (key_position >= 0))[:, None, None]
    scores = jnp.where(valid_mask, scores, NEGATIVE)
    sink_logit = sink_table.reshape(1, kv_heads, group_size, 1, 1)
    row_top = jnp.maximum(jnp.max(scores, axis=-1, keepdims=True), sink_logit)
    weights = jnp.where(valid_mask, jnp.exp(scores - row_top), 0.0)
    denominator = jnp.sum(weights, axis=-1, keepdims=True) + jnp.exp(sink_logit - row_top)
    probabilities = (weights / denominator).astype(jnp.bfloat16)
    attended = jnp.einsum(
        "nhgqk,nkhd->nqhgd", probabilities, value_band, preferred_element_type=jnp.float32
    )
    return attended.astype(jnp.bfloat16).reshape(row_count, kv_heads * group_size * HEAD)


def on_device(
    features,
    norm_gain,
    w_query,
    w_key,
    w_value,
    head_sinks,
    w_query_latent,
    w_kv_latent,
    w_rope_key,
    query_latent_gain,
    kv_latent_gain,
    w_query_content,
    w_query_rotary,
    w_key_up,
    w_value_up,
    w_branch_window,
    w_branch_latent,
    w_gate_window,
    w_gate_latent,
):
    tok_rows = features.shape[0]
    row_start = lax.axis_index("sp") * tok_rows
    row_end = row_start + tok_rows
    positions = row_start + jnp.arange(tok_rows, dtype=jnp.int32)
    gathered = lax.all_gather(features, "tp", axis=1, tiled=True)
    normed = rms_rows(gathered.astype(jnp.float32), norm_gain).astype(jnp.bfloat16)
    query_rows = project(normed, w_query).astype(jnp.bfloat16)
    key_rows = project(normed, w_key).astype(jnp.bfloat16)
    value_rows = project(normed, w_value).astype(jnp.bfloat16)
    key_width = key_rows.shape[1]
    packed = jnp.concatenate([key_rows, value_rows], axis=1)
    tail_rows = from_behind(packed[tok_rows - WINDOW :], "sp", 1)
    extended = jnp.concatenate([tail_rows, packed], axis=0)
    window_out = window_attention(
        query_rows, extended[:, :key_width], extended[:, key_width:], head_sinks, row_start
    )
    latent_query = rms_rows(project(normed, w_query_latent), query_latent_gain).astype(jnp.bfloat16)
    latent_kv = rms_rows(project(normed, w_kv_latent), kv_latent_gain).astype(jnp.bfloat16)
    rope_rows = rotate(project(normed, w_rope_key), positions).astype(jnp.bfloat16)
    lat_heads = w_key_up.shape[1] // NOPE
    query_content = (
        project(latent_query, w_query_content)
        .astype(jnp.bfloat16)
        .reshape(tok_rows, lat_heads, NOPE)
    )
    query_rotary = rotate(
        project(latent_query, w_query_rotary).reshape(tok_rows, lat_heads, ROPE), positions
    ).astype(jnp.bfloat16)
    scale_factor = (NOPE + ROPE) ** (-0.5)

    def attend(running, piece_keys, piece_values, rope_piece):
        running_max, denominator, accumulated = running
        piece_rows = piece_keys.shape[0]
        scores = (
            jnp.einsum(
                "qhd,khd->hqk",
                query_content,
                piece_keys.reshape(piece_rows, lat_heads, NOPE),
                preferred_element_type=jnp.float32,
            )
            + jnp.einsum(
                "qhr,kr->hqk", query_rotary, rope_piece, preferred_element_type=jnp.float32
            )
        ) * scale_factor
        key_position = jnp.arange(piece_rows, dtype=jnp.int32)
        live_mask = key_position[None, :] <= positions[:, None]
        scores = jnp.where(live_mask, scores, NEGATIVE)
        new_max = jnp.maximum(running_max, jnp.max(scores, axis=-1))
        weights = jnp.where(live_mask, jnp.exp(scores - new_max[..., None]), 0.0)
        denominator = jnp.sum(weights, axis=-1)
        accumulated = jnp.einsum(
            "hqk,khd->hqd",
            weights.astype(jnp.bfloat16),
            piece_values.reshape(piece_rows, lat_heads, VDIM),
            preferred_element_type=jnp.float32,
        )
        return (new_max, denominator, accumulated)

    initial = (
        jnp.full((lat_heads, tok_rows), NEGATIVE, jnp.float32),
        jnp.zeros((lat_heads, tok_rows), jnp.float32),
        jnp.zeros((lat_heads, tok_rows, VDIM), jnp.float32),
    )
    pieces = (
        lax.all_gather(latent_kv, "sp", axis=0, tiled=True),
        lax.all_gather(rope_rows, "sp", axis=0, tiled=True),
    )

    def compute(current):
        piece_keys = project(pieces[0], w_key_up).astype(jnp.bfloat16)
        piece_values = project(pieces[0], w_value_up).astype(jnp.bfloat16)
        return attend(current, piece_keys, piece_values, pieces[1])

    running = lax.cond(jnp.int32(0) < row_end, compute, lambda current: current, initial)
    latent_out = jnp.transpose(running[2] / running[1][..., None], (1, 0, 2))
    latent_out = latent_out.reshape(tok_rows, lat_heads * VDIM).astype(jnp.bfloat16)
    all_window, all_latent = (
        lax.all_gather(window_out, "tp", axis=1, tiled=True),
        lax.all_gather(latent_out, "tp", axis=1, tiled=True),
    )
    column_window, column_latent = (
        lax.all_to_all(w_branch_window, "tp", split_axis=1, concat_axis=0, tiled=True),
        lax.all_to_all(w_branch_latent, "tp", split_axis=1, concat_axis=0, tiled=True),
    )
    window_branch = project(all_window, column_window)
    latent_branch = project(all_latent, column_latent)
    window_gate = jax.nn.sigmoid(project(normed, w_gate_window))
    latent_gate = jax.nn.sigmoid(project(normed, w_gate_latent))
    return (window_gate * window_branch + latent_gate * latent_branch).astype(jnp.bfloat16)


def solution(mesh):
    return jax.shard_map(
        on_device,
        mesh=mesh,
        in_specs=(
            P("sp", "tp"),
            P(),
            P(None, "tp"),
            P(None, "tp"),
            P(None, "tp"),
            P("tp"),
            P(),
            P(),
            P(),
            P(),
            P(),
            P(None, "tp"),
            P(None, "tp"),
            P(None, "tp"),
            P(None, "tp"),
            P("tp", None),
            P("tp", None),
            P(None, "tp"),
            P(None, "tp"),
        ),
        out_specs=P("sp", "tp"),
        check_vma=False,
    )
```

profile of v0, /device:TPU:0, one launch (start us, length us, event | category | flops | bytes accessed | tf_op | source)
XLA Modules:
  0.0 168.1 jit_solution(3678124389484324087)
XLA Ops:
  7.3 2.3 %copy.60 = bf16[256,2048]{0,1:T(8,128)(2,1)} copy(bf16[256,2048]{1,0:T(8,128)(2,1)} %param.37) | data formatting | bytes 2097152 | tf_op args[16]
  9.5 4.4 %all-to-all-start.1 = ((bf16[256,4,512]{0,2,1:T(8,128)(2,1)}), bf16[256,4,512]{0,2,1:T(8,128)(2,1)S(1)}, u32[]{:S(2)}, u32[]{:S(2)}) async-start(bf16[256,4,512]{0,2,1:T(8,128)(2,1)} %bitcast.96), calls=%async_computation.1 | async-start | bytes 2097152 | tf_op jit(solution)/shard_map/all_to_all | solution.py:190
  14.0 2.3 %copy.57 = bf16[256,2048]{0,1:T(8,128)(2,1)} copy(bf16[256,2048]{1,0:T(8,128)(2,1)} %param.36) | data formatting | bytes 2097152 | tf_op args[15]
  16.3 19.8 %all-to-all-done.1 = bf16[256,4,512]{0,2,1:T(8,128)(2,1)S(1)} async-done(((bf16[256,4,512]{0,2,1:T(8,128)(2,1)}), bf16[256,4,512]{0,2,1:T(8,128)(2,1)S(1)}, u32[]{:S(2)}, u32[]{:S(2)}) %all-to-all-start.1) | async-done | bytes 1048608 | tf_op jit(solution)/shard_map/all_to_all | solution.py:190
  36.1 4.2 %all-to-all-start = ((bf16[256,4,512]{0,2,1:T(8,128)(2,1)}), bf16[256,4,512]{0,2,1:T(8,128)(2,1)}, u32[]{:S(2)}, u32[]{:S(2)}) async-start(bf16[256,4,512]{0,2,1:T(8,128)(2,1)} %bitcast.97), calls=%async_computation | async-start | bytes 2097152 | tf_op jit(solution)/shard_map/all_to_all | solution.py:189
  42.0 12.8 %all-to-all-done = bf16[256,4,512]{0,2,1:T(8,128)(2,1)} async-done(((bf16[256,4,512]{0,2,1:T(8,128)(2,1)}), bf16[256,4,512]{0,2,1:T(8,128)(2,1)}, u32[]{:S(2)}, u32[]{:S(2)}) %all-to-all-start) | async-done | bytes 1048608 | tf_op jit(solution)/shard_map/all_to_all | solution.py:189
  54.8 2.3 %copy.58 = bf16[4,256,512]{2,1,0:T(8,128)(2,1)} copy(bf16[4,256,512]{1,2,0:T(8,128)(2,1)} %bitcast.12) | data formatting | bytes 2097152 | tf_op jit(solution)/shard_map/all_to_all | solution.py:189
  57.1 1.9 %fusion.14 = f32[384]{0:T(512)S(1)} fusion(bf16[384,2048]{1,0:T(8,128)(2,1)} %all-gather.3.cloned.1.call-done), kind=kLoop, calls=%fused_computation.22 | loop fusion | flops 2358912 | bytes 1574400 | tf_op jit(solution)/shard_map/reduce_sum | solution.py:25
  61.7 2.0 %convolution_convert_fusion.6 = bf16[384,128]{0,1:T(8,128)(2,1)S(1)} fusion(bf16[384,2048]{1,0:T(8,128)(2,1)} %copy-done.2, bf16[2048,128]{1,0:T(8,128)(2,1)S(1)} %copy-done.12), kind=kOutput, calls=%fused_computation.46 | convolution fusion | flops 201375744 | bytes 2195456 | tf_op jit(solution)/shard_map/dot_general | solution.py:49
  63.8 2.0 %convolution_convert_fusion.5 = bf16[384,128]{0,1:T(8,128)(2,1)S(1)} fusion(bf16[384,2048]{1,0:T(8,128)(2,1)} %copy-done.2, bf16[2048,128]{1,0:T(8,128)(2,1)S(1)} %copy-done.13), kind=kOutput, calls=%fused_computation.45 | convolution fusion | flops 201375744 | bytes 2195456 | tf_op jit(solution)/shard_map/dot_general | solution.py:49
  66.5 5.2 %collective-permute-start = (bf16[128,256]{0,1:T(8,128)(2,1)}, bf16[128,256]{0,1:T(8,128)(2,1)}, u32[]{:S(2)}, u32[]{:S(2)}) collective-permute-start(bf16[128,256]{0,1:T(8,128)(2,1)} %pad_maximum_fusion.4), channel_id=1, source_target_pairs={{0,4},{4,8},{8,12},{12,16},{16,20},{20,24},{24,28},{1,5},{5,9},{9,... | collective-permute-start | bytes 196616 | tf_op jit(solution)/shard_map/ppermute | solution.py:19
  72.3 2.3 %convolution_convert_fusion.3 = bf16[384,256]{1,0:T(8,128)(2,1)S(1)} fusion(bf16[384,2048]{1,0:T(8,128)(2,1)} %copy-done.2, bf16[2048,256]{1,0:T(8,128)(2,1)} %param.23), kind=kOutput, calls=%fused_computation.42 | convolution fusion | flops 402751488 | bytes 2818048 | tf_op jit(solution)/shard_map/dot_general | solution.py:49
  74.9 2.1 %fusion.41 = f32[384,64]{0,1:T(8,128)S(1)} fusion(bf16[384,2048]{1,0:T(8,128)(2,1)} %copy-done.2, bf16[2048,64]{0,1:T(8,128)(2,1)S(1)} %copy-done.18), kind=kOutput, calls=%fused_computation.93 | convolution fusion | flops 100663296 | bytes 1933312 | tf_op jit(solution)/shard_map/dot_general | solution.py:49
  77.3 35.1 %all_gather.18 = bf16[3072,64]{0,1:T(8,128)(2,1)} all-gather(bf16[384,64]{0,1:T(8,128)(2,1)S(1)} %pad_maximum_fusion.5), channel_id=1, replica_groups=mesh['sp'=8,'tp'=4] {'sp'}, dimensions={0}, use_global_device_ids=true | all-gather | bytes 442368 | tf_op jit(solution)/shard_map/all_gather | solution.py:173
  112.5 2.7 %multiply_reduce_fusion = (f32[384]{0:T(512)S(1)}, f32[384,512]{1,0:T(8,128)S(1)}) fusion(bf16[384,2048]{1,0:T(8,128)(2,1)S(1)} %copy-done.3, bf16[2048,512]{1,0:T(8,128)(2,1)} %param.27), kind=kOutput, calls=%fused_computation.48 | convolution fusion | flops 805699200 | bytes 4457984 | tf_op jit(solution)/shard_map/dot_general | solution.py:49
  117.1 2.0 %fusion.24 = f32[384,512]{1,0:T(8,128)} fusion(bf16[384,2048]{1,0:T(8,128)(2,1)S(1)} %copy-done.3, bf16[2048,512]{1,0:T(8,128)(2,1)S(1)} %copy-done.24), kind=kOutput, calls=%fused_computation.39 | convolution fusion | flops 805896192 | bytes 4456448 | tf_op jit(solution)/shard_map/dot_general | solution.py:49
  119.1 2.0 %fusion.22 = f32[384,512]{1,0:T(8,128)} fusion(bf16[384,2048]{1,0:T(8,128)(2,1)S(1)} %copy-done.3, bf16[2048,512]{1,0:T(8,128)(2,1)S(1)} %copy-done.25), kind=kOutput, calls=%fused_computation.37 | convolution fusion | flops 805896192 | bytes 4456448 | tf_op jit(solution)/shard_map/dot_general | solution.py:49
  124.3 7.9 %all_gather.16 = bf16[384,1024]{0,1:T(8,128)(2,1)} all-gather(bf16[384,256]{0,1:T(8,128)(2,1)S(1)} %bitcast.100), channel_id=1, replica_groups=mesh['sp'=8,'tp'=4] {'tp'}, dimensions={1}, use_global_device_ids=true | all-gather | bytes 983040 | tf_op jit(solution)/shard_map/all_gather | solution.py:185
  132.2 15.7 %conditional.1 = (f32[2,384]{1,0:T(2,128)S(1)}, f32[2,384,128]{1,2,0:T(8,128)}) conditional(s32[]{:T(128)} %convert_element_type.75, () %tuple.13, (s32[]{:T(128)}, s32[384]{0:T(512)S(1)}, bf16[3072,512]{1,0:T(8,128)(2,1)}, bf16[512,256]{1,0:T(8,128)(2,1)S(1)}, bf16[384,256]{1,0:T(8,128)(2,1)}, /*index=5*/bf16[3072,64]{0,1:T(8,128)(2,1)}, ...), branch_computations={%region_5.6_spmd, %region_6.9_spmd} | conditional | flops 3146907136 | bytes 87218872 | solution.py:181
  133.1 3.4 %convolution_convert_fusion.1 = bf16[3072,256]{0,1:T(8,128)(2,1)S(1)} fusion(bf16[3072,512]{1,0:T(8,128)(2,1)} %get-tuple-element.26, bf16[512,256]{1,0:T(8,128)(2,1)S(1)} %get-tuple-element.38), kind=kOutput, calls=%fused_computation.12 | convolution fusion | flops 806092800 | bytes 4980736 | tf_op jit(solution)/shard_map/cond/branch_1_fun/dot_general | solution.py:49
  138.1 2.4 %fusion.39 = (f32[2,384]{1,0:T(2,128)S(1)}, f32[2,384,3072]{1,2,0:T(8,128)S(1)}) fusion(bf16[384,2,64]{0,2,1:T(8,128)(2,1)S(1)} %copy-done.14, bf16[3072,64]{0,1:T(8,128)(2,1)S(1)} %copy-done.9, f32[2,3072,384]{2,1,0:T(8,128)S(1)} %fusion.10, pred[384,3072]{0,1:T(8,128)(4,1)S(1)} %iota_compare_fusion), kind=kOutput, calls=%fused_computation.91 | convolution fusion | flops 311426304 | bytes 20548608 | tf_op jit(solution)/shard_map/cond/branch_1_fun/qhr,kr->hqk/dot_general | solution.py:148
  141.6 3.1 %fusion.4 = f32[2,384,128]{1,2,0:T(8,128)} fusion(bf16[3072,2,128]{0,2,1:T(8,128)(2,1)S(1)} %bitcast.93, f32[2,384,3072]{1,2,0:T(8,128)S(1)} %get-tuple-element.42, f32[2,384]{1,0:T(2,128)S(1)} %broadcast_maximum_fusion, pred[384,3072]{0,1:T(8,128)(4,1)S(1)} %iota_compare_fusion), kind=kOutput, calls=%fused_computation.6 | convolution fusion | flops 611057664 | bytes 12585984 | tf_op jit(solution)/shard_map/cond | solution.py:181
  144.7 3.2 %fusion.3 = f32[2,384]{1,0:T(2,128)S(1)} fusion(f32[2,384,3072]{1,2,0:T(8,128)S(1)} %get-tuple-element.42, f32[2,384]{1,0:T(2,128)S(1)} %broadcast_maximum_fusion, pred[384,3072]{0,1:T(8,128)(4,1)} %copy-done.4), kind=kLoop, calls=%fused_computation.5 | loop fusion | flops 7077120 | bytes 10622976 | tf_op jit(solution)/shard_map/cond/branch_1_fun/reduce_sum | solution.py:157
  149.0 9.0 %all_gather.19 = bf16[384,1024]{0,1:T(8,128)(2,1)S(1)} all-gather(bf16[384,256]{0,1:T(8,128)(2,1)S(1)} %bitcast.102), channel_id=1, replica_groups=mesh['sp'=8,'tp'=4] {'tp'}, dimensions={1}, use_global_device_ids=true | all-gather | bytes 983040 | tf_op jit(solution)/shard_map/all_gather | solution.py:186
  (109 shorter events, 19.9 us)
Async XLA Ops:
  6.5 53.0 %copy-start = (bf16[2048,512]{1,0:T(8,128)(2,1)S(1)}, bf16[2048,512]{1,0:T(8,128)(2,1)}, u32[]{:S(2)}) copy-start(bf16[2048,512]{1,0:T(8,128)(2,1)} %param.28) | copy-start | bytes 6291460
  6.5 50.6 %all-gather.3.cloned.1.call-start = ((), (), s32[]{:S(2)}) async-start(), calls=%async_computation.2 | async-start | bytes 1966080 | tf_op jit(solution)/shard_map/all_gather | solution.py:112
  9.5 4.4 %copy-start.26 = (f32[4]{0:T(128)S(1)}, f32[4]{0:T(128)}, u32[]{:S(2)}) copy-start(f32[4]{0:T(128)} %param.26) | copy-start | bytes 52
  9.5 26.6 %all-to-all-start.1 = ((bf16[256,4,512]{0,2,1:T(8,128)(2,1)}), bf16[256,4,512]{0,2,1:T(8,128)(2,1)S(1)}, u32[]{:S(2)}, u32[]{:S(2)}) async-start(bf16[256,4,512]{0,2,1:T(8,128)(2,1)} %bitcast.96), calls=%async_computation.1 | async-start | bytes 2097152 | tf_op jit(solution)/shard_map/all_to_all | solution.py:190
  36.1 18.7 %all-to-all-start = ((bf16[256,4,512]{0,2,1:T(8,128)(2,1)}), bf16[256,4,512]{0,2,1:T(8,128)(2,1)}, u32[]{:S(2)}, u32[]{:S(2)}) async-start(bf16[256,4,512]{0,2,1:T(8,128)(2,1)} %bitcast.97), calls=%async_computation | async-start | bytes 2097152 | tf_op jit(solution)/shard_map/all_to_all | solution.py:189
  40.3 91.8 %all-gather.5.cloned.1.call-start = ((), (), s32[]{:S(2)}) async-start(), calls=%async_computation.3 | async-start | bytes 3538944 | tf_op jit(solution)/shard_map/all_gather | solution.py:172
  54.8 4.2 %copy-start.21 = (f32[2048]{0:T(1024)S(1)}, f32[2048]{0:T(1024)}, u32[]{:S(2)}) copy-start(f32[2048]{0:T(1024)} %param.22) | copy-start | bytes 24580
  57.1 1.9 %copy-start.5 = (bf16[384,2048]{1,0:T(8,128)(2,1)S(1)}, bf16[384,2048]{1,0:T(8,128)(2,1)}, u32[]{:S(2)}) copy-start(bf16[384,2048]{1,0:T(8,128)(2,1)} %all-gather.3.cloned.1.call-done) | copy-start | bytes 4718596
  61.6 2.2 %copy-start.13 = (bf16[2048,128]{1,0:T(8,128)(2,1)S(1)}, bf16[2048,128]{1,0:T(8,128)(2,1)}, u32[]{:S(2)}) copy-start(bf16[2048,128]{1,0:T(8,128)(2,1)} %param.25) | copy-start | bytes 1572868
  66.5 55.2 %collective-permute-start = (bf16[128,256]{0,1:T(8,128)(2,1)}, bf16[128,256]{0,1:T(8,128)(2,1)}, u32[]{:S(2)}, u32[]{:S(2)}) collective-permute-start(bf16[128,256]{0,1:T(8,128)(2,1)} %pad_maximum_fusion.4), channel_id=1, source_target_pairs={{0,4},{4,8},{8,12},{12,16},{16,20},{20,24},{24,28},{1,5},{5,9},{9,... | collective-permute-start | bytes 196616 | tf_op jit(solution)/shard_map/ppermute | solution.py:19
  72.3 2.6 %copy-start.18 = (bf16[2048,64]{0,1:T(8,128)(2,1)S(1)}, bf16[2048,64]{0,1:T(8,128)(2,1)}, u32[]{:S(2)}) copy-start(bf16[2048,64]{0,1:T(8,128)(2,1)} %param.29) | copy-start | bytes 786436
  74.9 37.6 %copy-start.3 = (bf16[384,2048]{1,0:T(8,128)(2,1)S(1)}, bf16[384,2048]{1,0:T(8,128)(2,1)}, u32[]{:S(2)}) copy-start(bf16[384,2048]{1,0:T(8,128)(2,1)} %copy-done.2) | copy-start | bytes 4718596
  112.4 2.7 %copy-start.19 = (bf16[512,128]{1,0:T(8,128)(2,1)S(1)}, bf16[512,128]{1,0:T(8,128)(2,1)}, u32[]{:S(2)}) copy-start(bf16[512,128]{1,0:T(8,128)(2,1)} %param.33) | copy-start | bytes 393220
  112.4 2.7 %copy-start.22 = (f32[512]{0:T(512)S(1)}, f32[512]{0:T(512)}, u32[]{:S(2)}) copy-start(f32[512]{0:T(512)} %param.30) | copy-start | bytes 6148
  115.1 1.9 %copy-start.24 = (bf16[2048,512]{1,0:T(8,128)(2,1)S(1)}, bf16[2048,512]{1,0:T(8,128)(2,1)}, u32[]{:S(2)}) copy-start(bf16[2048,512]{1,0:T(8,128)(2,1)} %param.39) | copy-start | bytes 6291460
  117.1 2.0 %copy-start.25 = (bf16[2048,512]{1,0:T(8,128)(2,1)S(1)}, bf16[2048,512]{1,0:T(8,128)(2,1)}, u32[]{:S(2)}) copy-start(bf16[2048,512]{1,0:T(8,128)(2,1)} %param.38) | copy-start | bytes 6291460
  124.0 8.1 %copy-start.16 = (bf16[512,256]{1,0:T(8,128)(2,1)S(1)}, bf16[512,256]{1,0:T(8,128)(2,1)}, u32[]{:S(2)}) copy-start(bf16[512,256]{1,0:T(8,128)(2,1)} %param.34) | copy-start | bytes 786436
  133.1 8.5 %copy-start.4 = (pred[384,3072]{0,1:T(8,128)(4,1)}, pred[384,3072]{0,1:T(8,128)(4,1)S(1)}, u32[]{:S(2)}) copy-start(pred[384,3072]{0,1:T(8,128)(4,1)S(1)} %iota_compare_fusion) | copy-start | bytes 3538948 | tf_op jit(solution)/shard_map/cond
  133.1 3.4 %copy-start.11 = (bf16[384,256]{1,0:T(8,128)(2,1)S(1)}, bf16[384,256]{1,0:T(8,128)(2,1)}, u32[]{:S(2)}) copy-start(bf16[384,256]{1,0:T(8,128)(2,1)} %get-tuple-element.28) | copy-start | bytes 589828 | tf_op jit(solution)/shard_map/cond
  138.1 2.5 %copy-start.1 = (bf16[3072,512]{1,0:T(8,128)(2,1)S(1)}, bf16[3072,512]{1,0:T(8,128)(2,1)}, u32[]{:S(2)}) copy-start(bf16[3072,512]{1,0:T(8,128)(2,1)} %get-tuple-element.26) | copy-start | bytes 9437188 | tf_op jit(solution)/shard_map/cond
  138.1 2.5 %copy-start.17 = (bf16[512,256]{1,0:T(8,128)(2,1)S(1)}, bf16[512,256]{1,0:T(8,128)(2,1)}, u32[]{:S(2)}) copy-start(bf16[512,256]{1,0:T(8,128)(2,1)} %get-tuple-element.39) | copy-start | bytes 786436 | tf_op jit(solution)/shard_map/cond
  147.9 10.1 %copy-start.6 = (bf16[4,256,512]{2,1,0:T(8,128)(2,1)S(1)}, bf16[4,256,512]{2,1,0:T(8,128)(2,1)}, u32[]{:S(2)}) copy-start(bf16[4,256,512]{2,1,0:T(8,128)(2,1)} %copy.61) | copy-start | bytes 3145732
  158.0 1.9 %copy-start.8 = (bf16[384,1024]{0,1:T(8,128)(2,1)S(1)}, bf16[384,1024]{0,1:T(8,128)(2,1)}, u32[]{:S(2)}) copy-start(bf16[384,1024]{0,1:T(8,128)(2,1)} %all_gather.16) | copy-start | bytes 2359300
  158.0 1.9 %copy-start.10 = (f32[384,512]{1,0:T(8,128)S(1)}, f32[384,512]{1,0:T(8,128)}, u32[]{:S(2)}) copy-start(f32[384,512]{1,0:T(8,128)} %fusion.22) | copy-start | bytes 2359300
  (8 other events, 11.0 us)
Sparse Core Ops, SparseCore 0:
  8.9 29.3 all-gather.2
  61.7 65.5 all-gather.4
where the time goes:
time: 169 us; the launch traced here: 168 us
  blocking collectives  52 us (31%)
  waiting for transfers between devices  33.3 us (20%)
  matrix products  33.2 us (20%)
  starting transfers between devices  13.9 us (8%)
  between operations  13.7 us (8%)
  other arithmetic  11.6 us (7%)
  local copies, waits for them, and re-layouts  10.3 us (6%)
    all_gather x1, blocking collectives, on_device(): lax.all_gather(rope_rows, 'sp', axis=0, tiled=True)  35.1 us
    dot_general x14, matrix products, project(): return jnp.dot(left, right, preferred_element_type=jnp.float32)  25.1 us
    all_to_all x1, waiting for transfers between devices, on_device(): lax.all_to_all(w_branch_latent, 'tp', split_axis=1, concat_axis=0, tiled=...  19.8 us
    all_to_all x1, waiting for transfers between devices, on_device(): lax.all_to_all(w_branch_window, 'tp', split_axis=1, concat_axis=0, tiled=...  12.8 us
    all_gather x1, blocking collectives, on_device(): lax.all_gather(latent_out, 'tp', axis=1, tiled=True)  8.98 us
    all_gather x1, blocking collectives, on_device(): lax.all_gather(window_out, 'tp', axis=1, tiled=True)  7.89 us
    unnamed x45, local copies, waits for them, and re-layouts  5.36 us
    ppermute x1, starting transfers between devices, from_behind(): return lax.ppermute(shard, axis, pairs)  5.23 us
  transfers between devices with their start and end apart: 5, of which 2 were waited for; matrix products, arithmetic and copies ran while one was open for 18% of the time, Pallas kernels for 0%

commit v1 on v0

--- a/solution.py
+++ b/solution.py
@@ -11,6 +11,12 @@
 EPS = 1e-06
 THETA = 10000.0
 NEGATIVE = -1e30
+
+
+def gather_blocks(value, mesh_axis, along):
+    terms = lax.all_gather(value, mesh_axis, axis=0, tiled=False)
+    out = jnp.concatenate(terms, axis=along)
+    return out
 
 
 def from_behind(shard, axis, by):
@@ -183,7 +189,7 @@
     latent_out = latent_out.reshape(tok_rows, lat_heads * VDIM).astype(jnp.bfloat16)
     all_window, all_latent = (
         lax.all_gather(window_out, "tp", axis=1, tiled=True),
-        lax.all_gather(latent_out, "tp", axis=1, tiled=True),
+        gather_blocks(latent_out, "tp", 1),
     )
     column_window, column_latent = (
         lax.all_to_all(w_branch_window, "tp", split_axis=1, concat_axis=0, tiled=True),

time: 169 us -> 160 us (0.947)
  waiting for transfers between devices: 33.3 us -> 17.3 us
  local copies, waits for them, and re-layouts: 10.3 us -> 17 us
  other arithmetic: 11.6 us -> 9.37 us
  matrix products: 33.2 us -> 35 us
  blocking collectives: 52 us -> 53.8 us
    all_to_all x1, waiting for transfers between devices: 19.8 us -> 0.01 us  [on_device(): lax.all_to_all(w_branch_latent, 'tp', split_axis=1, concat_axis=0, tiled=...]
    all_to_all x1, waiting for transfers between devices: 12.8 us -> 16.6 us  [on_device(): lax.all_to_all(w_branch_window, 'tp', split_axis=1, concat_axis=0, tiled=...]
    dot_general x0 -> x1, matrix products: none -> 3.25 us  [attend(): jnp.einsum('hqk,khd->hqd', weights.astype(jnp.bfloat16), piece_values.res...]
    cond x1 -> x0, matrix products: 3.14 us -> none  [on_device(): lax.cond(jnp.int32(0) < row_end, compute, lambda current: current, initial)]
    slice x8, local copies, waits for them, and re-layouts: 0.83 us -> 3.69 us  [banded(): return jnp.concatenate([table[:-1], table[1:]], axis=1)]
    all_gather x1, blocking collectives: 7.89 us -> 9.62 us  [on_device(): lax.all_gather(window_out, 'tp', axis=1, tiled=True)]
    reshape x1, local copies, waits for them, and re-layouts: 0.2 us -> 1.91 us  [window_attention(): query_blocks = queries.reshape(blocks, WINDOW, kv_heads, group_size, HEAD)]
    unnamed x45 -> x39, local copies, waits for them, and re-layouts: 5.36 us -> 6.21 us
  transfers between devices with their start and end apart: 5 -> 5, of which waited for: 2 -> 1; matrix products, arithmetic and copies ran while one was open for 18% -> 35% of each run, Pallas kernels for 0% -> 0%
where the time goes in v1:
time: 160 us
  blocking collectives  53.8 us (34%)
  matrix products  35 us (22%)
  waiting for transfers between devices  17.3 us (11%)
  local copies, waits for them, and re-layouts  17 us (11%)
  between operations  13.7 us (9%)
  starting transfers between devices  13.2 us (8%)
  other arithmetic  9.37 us (6%)
    all_gather x1, blocking collectives, on_device(): lax.all_gather(rope_rows, 'sp', axis=0, tiled=True)  35 us
    dot_general x14, matrix products, project(): return jnp.dot(left, right, preferred_element_type=jnp.float32)  25.8 us
    all_to_all x1, waiting for transfers between devices, on_device(): lax.all_to_all(w_branch_window, 'tp', split_axis=1, concat_axis=0, tiled=...  16.6 us
    all_gather x1, blocking collectives, on_device(): lax.all_gather(window_out, 'tp', axis=1, tiled=True)  9.62 us
    all_gather x1, blocking collectives, gather_blocks(): terms = lax.all_gather(value, mesh_axis, axis=0, tiled=False)  9.16 us
    unnamed x39, local copies, waits for them, and re-layouts  6.21 us
    ppermute x1, starting transfers between devices, from_behind(): return lax.ppermute(shard, axis, pairs)  5.24 us
    all_to_all x1, starting transfers between devices, on_device(): lax.all_to_all(w_branch_window, 'tp', split_axis=1, concat_axis=0, tiled=...  4.4 us
  transfers between devices with their start and end apart: 5, of which 1 were waited for; matrix products, arithmetic and copies ran while one was open for 35% of the time, Pallas kernels for 0%

profile of v1, /device:TPU:0, one launch (start us, length us, event | category | flops | bytes accessed | tf_op | source)
XLA Modules:
  0.0 159.5 jit_solution(5919487533344396692)
XLA Ops:
  7.3 2.3 %copy.77 = bf16[256,2048]{0,1:T(8,128)(2,1)} copy(bf16[256,2048]{1,0:T(8,128)(2,1)} %param.36) | data formatting | bytes 2097152 | tf_op args[15]
  9.5 4.4 %all-to-all-start = ((bf16[256,4,512]{0,2,1:T(8,128)(2,1)}), bf16[256,4,512]{0,2,1:T(8,128)(2,1)S(1)}, u32[]{:S(2)}, u32[]{:S(2)}) async-start(bf16[256,4,512]{0,2,1:T(8,128)(2,1)} %bitcast.100), calls=%async_computation | async-start | bytes 2097152 | tf_op jit(solution)/shard_map/all_to_all | solution.py:195
  14.0 2.3 %copy.80 = bf16[256,2048]{0,1:T(8,128)(2,1)} copy(bf16[256,2048]{1,0:T(8,128)(2,1)} %param.37) | data formatting | bytes 2097152 | tf_op args[16]
  16.3 2.3 %copy.81 = bf16[256,4,512]{2,0,1:T(8,128)(2,1)} copy(bf16[256,4,512]{0,2,1:T(8,128)(2,1)} %bitcast.101) | data formatting | bytes 2097152 | tf_op jit(solution)/shard_map/all_to_all | solution.py:196
  19.5 16.6 %all-to-all-done = bf16[256,4,512]{0,2,1:T(8,128)(2,1)S(1)} async-done(((bf16[256,4,512]{0,2,1:T(8,128)(2,1)}), bf16[256,4,512]{0,2,1:T(8,128)(2,1)S(1)}, u32[]{:S(2)}, u32[]{:S(2)}) %all-to-all-start) | async-done | bytes 1048608 | tf_op jit(solution)/shard_map/all_to_all | solution.py:195
  37.0 3.5 %all-to-all-start.1 = ((bf16[256,4,512]{2,0,1:T(8,128)(2,1)}), bf16[256,4,512]{2,0,1:T(8,128)(2,1)S(1)}, u32[]{:S(2)}, u32[]{:S(2)}) async-start(bf16[256,4,512]{2,0,1:T(8,128)(2,1)} %copy.81), calls=%async_computation.1 | async-start | bytes 2097152 | tf_op jit(solution)/shard_map/all_to_all | solution.py:196
  40.6 2.3 %copy.78 = bf16[4,256,512]{2,1,0:T(8,128)(2,1)} copy(bf16[4,256,512]{1,2,0:T(8,128)(2,1)} %bitcast.99) | data formatting | bytes 2097152 | tf_op jit(solution)/shard_map/all_to_all | solution.py:195
  47.4 2.1 %convolution_convert_fusion.6 = bf16[384,128]{0,1:T(8,128)(2,1)S(1)} fusion(bf16[384,2048]{1,0:T(8,128)(2,1)} %copy-done.2, bf16[2048,128]{1,0:T(8,128)(2,1)} %param.24), kind=kOutput, calls=%fused_computation.47 | convolution fusion | flops 201375744 | bytes 2195456 | tf_op jit(solution)/shard_map/dot_general | solution.py:55
  50.2 2.1 %convolution_convert_fusion.5 = bf16[384,128]{0,1:T(8,128)(2,1)S(1)} fusion(bf16[384,2048]{1,0:T(8,128)(2,1)} %copy-done.2, bf16[2048,128]{1,0:T(8,128)(2,1)} %param.25), kind=kOutput, calls=%fused_computation.46 | convolution fusion | flops 201375744 | bytes 2195456 | tf_op jit(solution)/shard_map/dot_general | solution.py:55
  52.3 5.2 %collective-permute-start = (bf16[128,256]{0,1:T(8,128)(2,1)S(1)}, bf16[128,256]{0,1:T(8,128)(2,1)}, u32[]{:S(2)}, u32[]{:S(2)}) collective-permute-start(bf16[128,256]{0,1:T(8,128)(2,1)S(1)} %pad_maximum_fusion.4), channel_id=1, source_target_pairs={{0,4},{4,8},{8,12},{12,16},{16,20},{20,24},{24,28},{1,5},{5,9},{9,... | collective-permute-start | bytes 196616 | tf_op jit(solution)/shard_map/ppermute | solution.py:25
  59.1 3.0 %convolution_convert_fusion.3 = bf16[384,256]{1,0:T(8,128)(2,1)} fusion(bf16[384,2048]{1,0:T(8,128)(2,1)} %copy-done.2, bf16[2048,256]{1,0:T(8,128)(2,1)} %param.23), kind=kOutput, calls=%fused_computation.43 | convolution fusion | flops 402751488 | bytes 2818048 | tf_op jit(solution)/shard_map/dot_general | solution.py:55
  62.1 1.9 %reshape.226 = bf16[3,128,2,2,64]{4,3,2,1,0:T(2,128)(2,1)} reshape(bf16[384,256]{1,0:T(8,128)(2,1)} %convolution_convert_fusion.3) | data formatting | bytes 393216 | tf_op jit(solution)/shard_map/reshape | solution.py:63
  64.7 2.0 %fusion.45 = f32[384,64]{0,1:T(8,128)S(1)} fusion(bf16[384,2048]{1,0:T(8,128)(2,1)} %copy-done.2, bf16[2048,64]{0,1:T(8,128)(2,1)} %param.29), kind=kOutput, calls=%fused_computation.97 | convolution fusion | flops 100663296 | bytes 1933312 | tf_op jit(solution)/shard_map/dot_general | solution.py:55
  67.0 35.0 %all_gather.19 = bf16[3072,64]{0,1:T(8,128)(2,1)} all-gather(bf16[384,64]{0,1:T(8,128)(2,1)S(1)} %pad_maximum_fusion.5), channel_id=1, replica_groups=mesh['sp'=8,'tp'=4] {'sp'}, dimensions={0}, use_global_device_ids=true | all-gather | bytes 442368 | tf_op jit(solution)/shard_map/all_gather | solution.py:179
  102.1 2.7 %multiply_reduce_fusion = (f32[384]{0:T(512)S(1)}, f32[384,512]{1,0:T(8,128)S(1)}) fusion(bf16[384,2048]{1,0:T(8,128)(2,1)S(1)} %copy-done.3, bf16[2048,512]{1,0:T(8,128)(2,1)} %param.27), kind=kOutput, calls=%fused_computation.51 | convolution fusion | flops 805699200 | bytes 4457984 | tf_op jit(solution)/shard_map/dot_general | solution.py:55
  106.8 2.0 %fusion.25 = f32[384,512]{1,0:T(8,128)} fusion(bf16[384,2048]{1,0:T(8,128)(2,1)S(1)} %copy-done.3, bf16[2048,512]{1,0:T(8,128)(2,1)S(1)} %copy-done.20), kind=kOutput, calls=%fused_computation.40 | convolution fusion | flops 805896192 | bytes 4456448 | tf_op jit(solution)/shard_map/dot_general | solution.py:55
  108.8 2.0 %fusion.23 = f32[384,512]{1,0:T(8,128)} fusion(bf16[384,2048]{1,0:T(8,128)(2,1)S(1)} %copy-done.3, bf16[2048,512]{1,0:T(8,128)(2,1)S(1)} %copy-done.21), kind=kOutput, calls=%fused_computation.38 | convolution fusion | flops 805896192 | bytes 4456448 | tf_op jit(solution)/shard_map/dot_general | solution.py:55
  115.8 9.6 %all_gather.17 = bf16[384,1024]{0,1:T(8,128)(2,1)} all-gather(bf16[384,256]{0,1:T(8,128)(2,1)S(1)} %bitcast.104), channel_id=1, replica_groups=mesh['sp'=8,'tp'=4] {'tp'}, dimensions={1}, use_global_device_ids=true | all-gather | bytes 983040 | tf_op jit(solution)/shard_map/all_gather | solution.py:191
  125.4 14.1 %conditional.1 = (f32[2,384]{1,0:T(2,128)S(1)}, f32[2,384,128]{2,1,0:T(8,128)S(1)}) conditional(s32[]{:T(128)} %convert_element_type.82, () %tuple.13, (s32[]{:T(128)}, s32[384]{0:T(512)S(1)}, bf16[3072,512]{1,0:T(8,128)(2,1)}, bf16[512,256]{1,0:T(8,128)(2,1)}, bf16[384,256]{1,0:T(8,128)(2,1)}, /*index=5*/bf16[3072,64]{0,1:T(8,128)(2,1)}, ...), branch_computations={%region_5.6_spmd, %region_6.9_spmd} | conditional | flops 3146907136 | bytes 82500256 | solution.py:187
  126.3 3.0 %convolution_convert_fusion.1 = bf16[3072,256]{0,1:T(8,128)(2,1)S(1)} fusion(bf16[3072,512]{1,0:T(8,128)(2,1)} %get-tuple-element.26, bf16[512,256]{1,0:T(8,128)(2,1)} %get-tuple-element.38), kind=kOutput, calls=%fused_computation.12 | convolution fusion | flops 806092800 | bytes 4980736 | tf_op jit(solution)/shard_map/cond/branch_1_fun/dot_general | solution.py:55
  130.9 2.4 %fusion.43 = (f32[2,384]{1,0:T(2,128)S(1)}, f32[2,384,3072]{1,2,0:T(8,128)S(1)}) fusion(bf16[384,2,64]{0,2,1:T(8,128)(2,1)S(1)} %copy-done.11, bf16[3072,64]{0,1:T(8,128)(2,1)S(1)} %copy-done.8, f32[2,3072,384]{2,1,0:T(8,128)S(1)} %fusion.10, pred[384,3072]{0,1:T(8,128)(4,1)S(1)} %iota_compare_fusion), kind=kOutput, calls=%fused_computation.95 | convolution fusion | flops 311426304 | bytes 20548608 | tf_op jit(solution)/shard_map/cond/branch_1_fun/qhr,kr->hqk/dot_general | solution.py:154
  134.4 3.2 %fusion.4 = f32[2,384,128]{2,1,0:T(8,128)S(1)} fusion(bf16[3072,2,128]{0,2,1:T(8,128)(2,1)S(1)} %bitcast.98, f32[2,384,3072]{1,2,0:T(8,128)S(1)} %get-tuple-element.41, f32[2,384]{1,0:T(2,128)S(1)} %broadcast_maximum_fusion, pred[384,3072]{0,1:T(8,128)(4,1)S(1)} %iota_compare_fusion), kind=kOutput, calls=%fused_computation.6 | convolution fusion | flops 611057664 | bytes 12585984 | tf_op jit(solution)/shard_map/cond/branch_1_fun/hqk,khd->hqd/dot_general | solution.py:164
  140.0 9.2 %all_gather.20 = bf16[4,384,256]{2,1,0:T(8,128)(2,1)} all-gather(bf16[1,384,256]{2,1,0:T(8,128)(2,1)S(1)} %convert_element_type.89), channel_id=1, replica_groups=mesh['sp'=8,'tp'=4] {'tp'}, dimensions={0}, use_global_device_ids=true | all-gather | bytes 983040 | tf_op jit(solution)/shard_map/all_gather | solution.py:17
  149.2 2.1 %fusion.20 = f32[384,512]{1,0:T(8,128)S(1)} fusion(f32[384,512]{1,0:T(8,128)} %fusion.25, bf16[256,4,512]{2,0,1:T(8,128)(2,1)S(1)} %all-to-all-done.1, bf16[4,384,256]{2,1,0:T(8,128)(2,1)} %all_gather.20), kind=kOutput, calls=%fused_computation.35 | convolution fusion | flops 402849792 | bytes 3407872 | tf_op jit(solution)/shard_map/dot_general | solution.py:55
  (103 shorter events, 24.6 us)
Async XLA Ops:
  6.5 38.8 %copy-start = (bf16[2048,512]{1,0:T(8,128)(2,1)S(1)}, bf16[2048,512]{1,0:T(8,128)(2,1)}, u32[]{:S(2)}) copy-start(bf16[2048,512]{1,0:T(8,128)(2,1)} %param.28) | copy-start | bytes 6291460
  6.5 36.4 %all-gather.3.cloned.1.call-start = ((), (), s32[]{:S(2)}) async-start(), calls=%async_computation.2 | async-start | bytes 1966080 | tf_op jit(solution)/shard_map/all_gather | solution.py:118
  9.5 4.4 %copy-start.22 = (f32[4]{0:T(128)S(1)}, f32[4]{0:T(128)}, u32[]{:S(2)}) copy-start(f32[4]{0:T(128)} %param.26) | copy-start | bytes 52
  9.5 26.5 %all-to-all-start = ((bf16[256,4,512]{0,2,1:T(8,128)(2,1)}), bf16[256,4,512]{0,2,1:T(8,128)(2,1)S(1)}, u32[]{:S(2)}, u32[]{:S(2)}) async-start(bf16[256,4,512]{0,2,1:T(8,128)(2,1)} %bitcast.100), calls=%async_computation | async-start | bytes 2097152 | tf_op jit(solution)/shard_map/all_to_all | solution.py:195
  37.0 112.1 %all-to-all-start.1 = ((bf16[256,4,512]{2,0,1:T(8,128)(2,1)}), bf16[256,4,512]{2,0,1:T(8,128)(2,1)S(1)}, u32[]{:S(2)}, u32[]{:S(2)}) async-start(bf16[256,4,512]{2,0,1:T(8,128)(2,1)} %copy.81), calls=%async_computation.1 | async-start | bytes 2097152 | tf_op jit(solution)/shard_map/all_to_all | solution.py:196
  40.6 84.8 %all-gather.5.cloned.1.call-start = ((), (), s32[]{:S(2)}) async-start(), calls=%async_computation.3 | async-start | bytes 3538944 | tf_op jit(solution)/shard_map/all_gather | solution.py:178
  40.6 4.2 %copy-start.17 = (f32[2048]{0:T(1024)S(1)}, f32[2048]{0:T(1024)}, u32[]{:S(2)}) copy-start(f32[2048]{0:T(1024)} %param.22) | copy-start | bytes 24580
  42.9 1.9 %copy-start.4 = (bf16[384,2048]{1,0:T(8,128)(2,1)S(1)}, bf16[384,2048]{1,0:T(8,128)(2,1)}, u32[]{:S(2)}) copy-start(bf16[384,2048]{1,0:T(8,128)(2,1)} %all-gather.3.cloned.1.call-done) | copy-start | bytes 4718596
  52.3 59.1 %collective-permute-start = (bf16[128,256]{0,1:T(8,128)(2,1)S(1)}, bf16[128,256]{0,1:T(8,128)(2,1)}, u32[]{:S(2)}, u32[]{:S(2)}) collective-permute-start(bf16[128,256]{0,1:T(8,128)(2,1)S(1)} %pad_maximum_fusion.4), channel_id=1, source_target_pairs={{0,4},{4,8},{8,12},{12,16},{16,20},{20,24},{24,28},{1,5},{5,9},{9,... | collective-permute-start | bytes 196616 | tf_op jit(solution)/shard_map/ppermute | solution.py:25
  64.1 38.0 %copy-start.3 = (bf16[384,2048]{1,0:T(8,128)(2,1)S(1)}, bf16[384,2048]{1,0:T(8,128)(2,1)}, u32[]{:S(2)}) copy-start(bf16[384,2048]{1,0:T(8,128)(2,1)} %copy-done.2) | copy-start | bytes 4718596
  102.1 2.7 %copy-start.15 = (bf16[512,128]{1,0:T(8,128)(2,1)S(1)}, bf16[512,128]{1,0:T(8,128)(2,1)}, u32[]{:S(2)}) copy-start(bf16[512,128]{1,0:T(8,128)(2,1)} %param.33) | copy-start | bytes 393220
  102.1 2.7 %copy-start.18 = (f32[512]{0:T(512)S(1)}, f32[512]{0:T(512)}, u32[]{:S(2)}) copy-start(f32[512]{0:T(512)} %param.30) | copy-start | bytes 6148
  104.8 2.0 %copy-start.20 = (bf16[2048,512]{1,0:T(8,128)(2,1)S(1)}, bf16[2048,512]{1,0:T(8,128)(2,1)}, u32[]{:S(2)}) copy-start(bf16[2048,512]{1,0:T(8,128)(2,1)} %param.39) | copy-start | bytes 6291460
  106.8 2.0 %copy-start.21 = (bf16[2048,512]{1,0:T(8,128)(2,1)S(1)}, bf16[2048,512]{1,0:T(8,128)(2,1)}, u32[]{:S(2)}) copy-start(bf16[2048,512]{1,0:T(8,128)(2,1)} %param.38) | copy-start | bytes 6291460
  112.3 2.4 %copy-start.12 = (pred[3,128,256]{1,2,0:T(8,128)(4,1)S(1)}, pred[3,128,256]{1,2,0:T(8,128)(4,1)}, u32[]{:S(2)}) copy-start(pred[3,128,256]{1,2,0:T(8,128)(4,1)} %broadcast_and_fusion) | copy-start | bytes 294916
  113.0 2.1 %copy-start.16 = (bf16[3,128,2,64]{1,3,2,0:T(8,128)(2,1)S(1)}, bf16[3,128,2,64]{1,3,2,0:T(8,128)(2,1)}, u32[]{:S(2)}) copy-start(bf16[3,128,2,64]{1,3,2,0:T(8,128)(2,1)} %copy.70) | copy-start | bytes 294916
  126.3 3.0 %copy-start.10 = (bf16[384,256]{1,0:T(8,128)(2,1)S(1)}, bf16[384,256]{1,0:T(8,128)(2,1)}, u32[]{:S(2)}) copy-start(bf16[384,256]{1,0:T(8,128)(2,1)} %get-tuple-element.28) | copy-start | bytes 589828 | tf_op jit(solution)/shard_map/cond
  129.3 1.6 %copy-start.8 = (bf16[3072,64]{0,1:T(8,128)(2,1)S(1)}, bf16[3072,64]{0,1:T(8,128)(2,1)}, u32[]{:S(2)}) copy-start(bf16[3072,64]{0,1:T(8,128)(2,1)} %get-tuple-element.29) | copy-start | bytes 1179652 | tf_op jit(solution)/shard_map/cond
  129.3 1.6 %copy-start.11 = (bf16[384,2,64]{0,2,1:T(8,128)(2,1)S(1)}, bf16[384,2,64]{0,2,1:T(8,128)(2,1)}, u32[]{:S(2)}) copy-start(bf16[384,2,64]{0,2,1:T(8,128)(2,1)} %get-tuple-element.30) | copy-start | bytes 294916 | tf_op jit(solution)/shard_map/cond
  130.9 2.4 %copy-start.1 = (bf16[3072,512]{1,0:T(8,128)(2,1)S(1)}, bf16[3072,512]{1,0:T(8,128)(2,1)}, u32[]{:S(2)}) copy-start(bf16[3072,512]{1,0:T(8,128)(2,1)} %get-tuple-element.26) | copy-start | bytes 9437188 | tf_op jit(solution)/shard_map/cond
  130.9 2.4 %copy-start.14 = (bf16[512,256]{1,0:T(8,128)(2,1)S(1)}, bf16[512,256]{1,0:T(8,128)(2,1)}, u32[]{:S(2)}) copy-start(bf16[512,256]{1,0:T(8,128)(2,1)} %get-tuple-element.39) | copy-start | bytes 786436 | tf_op jit(solution)/shard_map/cond
  149.2 2.1 %copy-start.6 = (bf16[4,256,512]{2,1,0:T(8,128)(2,1)S(1)}, bf16[4,256,512]{2,1,0:T(8,128)(2,1)}, u32[]{:S(2)}) copy-start(bf16[4,256,512]{2,1,0:T(8,128)(2,1)} %copy.78) | copy-start | bytes 3145732
  149.2 2.1 %copy-start.7 = (bf16[384,1024]{0,1:T(8,128)(2,1)S(1)}, bf16[384,1024]{0,1:T(8,128)(2,1)}, u32[]{:S(2)}) copy-start(bf16[384,1024]{0,1:T(8,128)(2,1)} %all_gather.17) | copy-start | bytes 2359300
  149.2 2.2 %copy-start.9 = (f32[384,512]{1,0:T(8,128)S(1)}, f32[384,512]{1,0:T(8,128)}, u32[]{:S(2)}) copy-start(f32[384,512]{1,0:T(8,128)} %fusion.23) | copy-start | bytes 2359300
  (4 other events, 4.3 us)
Sparse Core Ops, SparseCore 0:
  8.9 29.3 all-gather.2
  47.5 67.1 all-gather.4
